TPU v7x, 32 devices: a whole 2x2x4 slice. The times are simulated.
32 devices in a mesh: st: 16 (over z, y, x), tp: 2 (over core).
Axes of the slice: x: 2, y: 2, z: 4, core: 2. Of those that a mesh axis runs over, the one named last changes fastest.
Arguments:
- hidden: bfloat16 [8192, 2048], P('st'), may hold values from -24 to 24
- passage_store: bfloat16 [512, 64, 2048], P('st'), may hold values from -6 to 6
- passage_ids: int32 [128, 4], P('st'), may hold values from 0 to 511, as said below
- query_weight: bfloat16 [2048, 512], P(None, 'tp'), may hold values from -0.125 to 0.125
- gate_weight: bfloat16 [2048, 512], P(None, 'tp'), may hold values from -0.125 to 0.125
- key_weight: bfloat16 [2048, 512], P(None, 'tp'), may hold values from -0.125 to 0.125
- value_weight: bfloat16 [2048, 512], P(None, 'tp'), may hold values from -0.125 to 0.125
- output_grad: bfloat16 [8192, 512], P('st', 'tp'), may hold values from -6 to 6
Outputs:
- grad_hidden: bfloat16 [8192, 2048], P(('st', 'tp'))
- grad_store: bfloat16 [512, 64, 2048], P(('st', 'tp'))
- grad_value_weight: float32 [2048, 512], P(None, 'tp')
Inputs may be any that keep to these rules, and one draw needn't show every extreme that they name: `passage_ids`: passage p is held at st index p // 32. The 32 ids of one index of st (its 8 blocks) are distinct; at most 4 of them name passages of one owner, and on every index some owner is named exactly 4 times. Every index reads at least one passage of the owner before it, of the owner after it and of the owner half the axis away.
All inputs are finite; a program needn't handle non-finite values.
Results may differ from a plain program's by a relative error of at most 0.012.
The roundings to bfloat16 on the way count: a program that leaves them out, or rounds other values in their place, can miss the bound.
Values may be sent and summed in bfloat16 or wider, within the bound.
A program may use at most 128 MiB of HBM per device.

v0:
```python
import jax
import jax.numpy as jnp
from jax import lax
from jax.sharding import PartitionSpec as P

HEAD_DIM = 256


def body(
    hidden,
    passage_store,
    passage_ids,
    query_weight,
    gate_weight,
    key_weight,
    value_weight,
    output_grad,
):
    owner_count = lax.axis_size("st")
    own_index = lax.axis_index("st")
    held_count = passage_store.shape[0]
    span_rows = passage_store.shape[1]
    model_width = passage_store.shape[2]
    block_count = passage_ids.shape[0]
    per_block = passage_ids.shape[1]
    requests = block_count * per_block
    capacity = max(1, 2 * requests // owner_count)
    local_width = query_weight.shape[1]
    local_heads = local_width // HEAD_DIM
    tokens_here = hidden.shape[0]
    block_rows = tokens_here // block_count
    all_ids = lax.all_gather(passage_ids, "st", axis=0, tiled=True).reshape(owner_count, requests)
    owner_of = all_ids // held_count
    local_index = all_ids % held_count
    positions = jnp.arange(requests, dtype=jnp.int32)
    earlier = positions[None, :] < positions[:, None]
    matching = owner_of[:, :, None] == owner_of[:, None, :]
    slot_rank = jnp.sum(matching & earlier[None], axis=2)
    slot_iota = jnp.arange(capacity, dtype=jnp.int32)
    placed = (owner_of == own_index)[:, :, None] & (
        slot_rank[:, :, None] == slot_iota[None, None, :]
    )
    slot_table = jnp.sum(jnp.where(placed, local_index[:, :, None], 0), axis=1)
    filled = jnp.any(placed, axis=1)
    my_owner = lax.dynamic_index_in_dim(owner_of, own_index, 0, keepdims=False)
    my_rank = lax.dynamic_index_in_dim(slot_rank, own_index, 0, keepdims=False)
    slot_flat = my_owner * capacity + my_rank
    store_rows = passage_store.reshape(held_count * span_rows, model_width)
    keys_here = (
        jnp.dot(store_rows, key_weight, preferred_element_type=jnp.float32)
        .astype(jnp.bfloat16)
        .reshape(held_count, span_rows, local_width)
    )
    values_here = (
        jnp.dot(store_rows, value_weight, preferred_element_type=jnp.float32)
        .astype(jnp.bfloat16)
        .reshape(held_count, span_rows, local_width)
    )
    came_keys, came_values = (
        lax.all_to_all(keys_here[slot_table], "st", split_axis=0, concat_axis=0, tiled=True),
        lax.all_to_all(values_here[slot_table], "st", split_axis=0, concat_axis=0, tiled=True),
    )
    got_keys = came_keys.reshape(owner_count * capacity, span_rows, local_width)[slot_flat]
    got_values = came_values.reshape(owner_count * capacity, span_rows, local_width)[slot_flat]
    key_heads = got_keys.reshape(block_count, per_block * span_rows, local_heads, HEAD_DIM)
    value_heads = got_values.reshape(block_count, per_block * span_rows, local_heads, HEAD_DIM)
    queries = jnp.dot(hidden, query_weight, preferred_element_type=jnp.float32).astype(jnp.bfloat16)
    gates = jnp.dot(hidden, gate_weight, preferred_element_type=jnp.float32)
    query_heads = queries.reshape(block_count, block_rows, local_heads, HEAD_DIM)
    score_scale = HEAD_DIM ** (-0.5)
    scores = (
        jnp.einsum("bqhd,bkhd->bhqk", query_heads, key_heads, preferred_element_type=jnp.float32)
        * score_scale
    )
    probs = jax.nn.softmax(scores, axis=-1)
    probs_low = probs.astype(jnp.bfloat16)
    attended = jnp.einsum(
        "bhqk,bkhd->bqhd", probs_low, value_heads, preferred_element_type=jnp.float32
    ).reshape(tokens_here, local_width)
    gate_sigmoid = jax.nn.sigmoid(gates)
    upstream = output_grad.astype(jnp.float32)
    d_attended = (upstream * gates * gate_sigmoid).astype(jnp.bfloat16)
    d_gates = (upstream * attended * gate_sigmoid * (1.0 + gates * (1.0 - gate_sigmoid))).astype(
        jnp.bfloat16
    )
    d_heads = d_attended.reshape(block_count, block_rows, local_heads, HEAD_DIM)
    d_probs = jnp.einsum(
        "bqhd,bkhd->bhqk", d_heads, value_heads, preferred_element_type=jnp.float32
    )
    centre = jnp.sum(probs * d_probs, axis=-1, keepdims=True)
    d_scores = (probs * (d_probs - centre) * score_scale).astype(jnp.bfloat16)
    d_queries = (
        jnp.einsum("bhqk,bkhd->bqhd", d_scores, key_heads, preferred_element_type=jnp.float32)
        .astype(jnp.bfloat16)
        .reshape(tokens_here, local_width)
    )
    d_block_keys = jnp.einsum(
        "bhqk,bqhd->bkhd", d_scores, query_heads, preferred_element_type=jnp.float32
    ).reshape(requests, span_rows, local_width)
    d_block_values = jnp.einsum(
        "bhqk,bqhd->bkhd", probs_low, d_heads, preferred_element_type=jnp.float32
    ).reshape(requests, span_rows, local_width)
    contract = (((1,), (1,)), ((), ()))
    slot_total = owner_count * capacity
    back_keys = (
        jnp.zeros((slot_total, span_rows, local_width), jnp.float32).at[slot_flat].set(d_block_keys)
    )
    back_values = (
        jnp.zeros((slot_total, span_rows, local_width), jnp.float32)
        .at[slot_flat]
        .set(d_block_values)
    )
    came_dkeys, came_dvalues = (
        lax.all_to_all(
            back_keys.reshape(owner_count, capacity, span_rows, local_width),
            "st",
            split_axis=0,
            concat_axis=0,
            tiled=True,
        ),
        lax.all_to_all(
            back_values.reshape(owner_count, capacity, span_rows, local_width),
            "st",
            split_axis=0,
            concat_axis=0,
            tiled=True,
        ),
    )
    slot_owner = jnp.where(filled, slot_table, -1).reshape(slot_total)
    selector = (jnp.arange(held_count, dtype=jnp.int32)[:, None] == slot_owner[None, :]).astype(
        jnp.float32
    )
    key_totals = jnp.dot(
        selector,
        came_dkeys.reshape(slot_total, span_rows * local_width),
        precision=lax.Precision.HIGHEST,
        preferred_element_type=jnp.float32,
    )
    value_totals = jnp.dot(
        selector,
        came_dvalues.reshape(slot_total, span_rows * local_width),
        precision=lax.Precision.HIGHEST,
        preferred_element_type=jnp.float32,
    )
    key_low = key_totals.astype(jnp.bfloat16).reshape(held_count, span_rows, local_width)
    value_low = value_totals.astype(jnp.bfloat16).reshape(held_count, span_rows, local_width)
    weight_part = lax.dot_general(
        store_rows,
        value_low.reshape(held_count * span_rows, local_width),
        (((0,), (0,)), ((), ())),
        preferred_element_type=jnp.float32,
    )
    grad_value_weight = lax.psum(weight_part, "st")
    grad_hidden = lax.psum_scatter(
        lax.dot_general(d_queries, query_weight, contract, preferred_element_type=jnp.float32)
        + lax.dot_general(d_gates, gate_weight, contract, preferred_element_type=jnp.float32),
        "tp",
        scatter_dimension=0,
        tiled=True,
    ).astype(jnp.bfloat16)
    rows_key = key_low.reshape(
        held_count // lax.axis_size("tp") * lax.axis_size("tp") * span_rows, local_width
    )
    rows_value = value_low.reshape(
        held_count // lax.axis_size("tp") * lax.axis_size("tp") * span_rows, local_width
    )
    summed = lax.dot_general(
        rows_key, key_weight, contract, preferred_element_type=jnp.float32
    ) + lax.dot_general(rows_value, value_weight, contract, preferred_element_type=jnp.float32)
    grad_store = lax.psum_scatter(
        summed.reshape(
            held_count // lax.axis_size("tp") * lax.axis_size("tp"), span_rows, model_width
        ),
        "tp",
        scatter_dimension=0,
        tiled=True,
    ).astype(jnp.bfloat16)
    return (grad_hidden, grad_store, grad_value_weight)


def solution(mesh):
    placed = (
        P("st", None),
        P("st", None, None),
        P("st", None),
        P(None, "tp"),
        P(None, "tp"),
        P(None, "tp"),
        P(None, "tp"),
        P("st", "tp"),
    )
    return jax.shard_map(
        body,
        mesh=mesh,
        in_specs=placed,
        out_specs=(P(("st", "tp"), None), P(("st", "tp"), None, None), P(None, "tp")),
        check_vma=False,
    )
```

profile of v0, /device:TPU:0, one launch (start us, length us, event | category | flops | bytes accessed | tf_op | source)
XLA Modules:
  0.0 531.6 jit_solution(4978605036159977339)
XLA Ops:
  8.0 42.9 %all-gather = s32[16,8,4]{1,2,0:T(4,128)S(1)} all-gather(s32[1,8,4]{1,2,0:T(4,128)} %bitcast.110), channel_id=1, replica_groups=mesh['st'=16,'tp'=2] {'st'}, dimensions={0}, use_global_device_ids=true | all-gather | bytes 2176 | tf_op jit(solution)/shard_map/all_gather | solution.py:32
  51.2 0.5 convert_reduce_fusion
  51.6 0.2 select_reduce_fusion
  52.0 6.0 %convolution_convert_fusion.2 = bf16[2048,256]{1,0:T(8,128)(2,1)S(1)} fusion(bf16[2048,2048]{1,0:T(8,128)(2,1)} %bitcast.89, bf16[2048,256]{1,0:T(8,128)(2,1)} %param.14), kind=kOutput, calls=%fused_computation.13 | convolution fusion | flops 2148007936 | bytes 10485760 | tf_op jit(solution)/shard_map/dot_general | solution.py:55
  58.0 2.0 gather_fusion.2
  60.0 4.4 all-to-all-start.1
  64.4 6.0 %convolution_convert_fusion.3 = bf16[2048,256]{1,0:T(8,128)(2,1)S(1)} fusion(bf16[2048,2048]{1,0:T(8,128)(2,1)} %bitcast.90, bf16[2048,256]{1,0:T(8,128)(2,1)} %param.13), kind=kOutput, calls=%fused_computation.14 | convolution fusion | flops 2148007936 | bytes 10485760 | tf_op jit(solution)/shard_map/dot_general | solution.py:50
  70.4 2.0 gather_fusion
  72.4 30.7 %all-to-all-done.1 = bf16[16,4,64,256]{3,2,1,0:T(8,128)(2,1)} async-done(((bf16[16,4,64,256]{3,2,1,0:T(8,128)(2,1)}), bf16[16,4,64,256]{3,2,1,0:T(8,128)(2,1)}, u32[]{:S(2)}, u32[]{:S(2)}) %all-to-all-start.1) | async-done | bytes 2097184 | tf_op jit(solution)/shard_map/all_to_all | solution.py:61
  103.1 7.6 %all-to-all-start = ((bf16[16,4,64,256]{3,2,1,0:T(8,128)(2,1)}), bf16[16,4,64,256]{3,2,1,0:T(8,128)(2,1)}, u32[]{:S(2)}, u32[]{:S(2)}) async-start(bf16[16,4,64,256]{3,2,1,0:T(8,128)(2,1)} %bitcast.95), calls=%async_computation | async-start | bytes 4194304 | tf_op jit(solution)/shard_map/all_to_all | solution.py:60
  110.7 0.7 convolution_convert_fusion.5
  111.4 3.3 gather_fusion.3
  114.7 36.4 %all-to-all-done = bf16[16,4,64,256]{3,2,1,0:T(8,128)(2,1)} async-done(((bf16[16,4,64,256]{3,2,1,0:T(8,128)(2,1)}), bf16[16,4,64,256]{3,2,1,0:T(8,128)(2,1)}, u32[]{:S(2)}, u32[]{:S(2)}) %all-to-all-start) | async-done | bytes 2097184 | tf_op jit(solution)/shard_map/all_to_all | solution.py:60
  151.1 2.2 gather_fusion.1
  153.3 0.4 convolution_multiply_fusion
  153.8 0.8 copy-done.3
  154.5 0.9 fusion.35
  155.5 3.3 fusion.22
  158.8 3.1 fusion.17
  161.9 1.2 fusion.36
  163.1 4.9 fusion.8
  168.0 2.5 broadcast.191.clone
  170.6 5.3 %scatter_fusion = f32[64,64,256]{2,1,0:T(8,128)} fusion(f32[64,64,256]{2,1,0:T(8,128)} %broadcast.191.clone, s32[32]{0:T(128)S(1)} %fusion.30, f32[32,64,256]{2,1,0:T(8,128)S(1)} %bitcast.103), kind=kCustom, calls=%fused_computation.4 | custom fusion | bytes 6291584 | tf_op jit(solution)/shard_map/scatter | solution.py:106
  175.9 9.8 %all-to-all-start.2 = ((f32[16,4,64,256]{3,2,1,0:T(8,128)}), f32[16,4,64,256]{3,2,1,0:T(8,128)}, u32[]{:S(2)}, u32[]{:S(2)}) async-start(f32[16,4,64,256]{3,2,1,0:T(8,128)} %bitcast.88), calls=%async_computation.3 | async-start | bytes 8388608 | tf_op jit(solution)/shard_map/all_to_all | solution.py:114
  185.8 2.6 fusion.20
  188.3 2.5 broadcast.191.clone.1
  190.8 5.5 %scatter_fusion.1 = f32[64,64,256]{2,1,0:T(8,128)} fusion(f32[64,64,256]{2,1,0:T(8,128)} %broadcast.191.clone.1, s32[32]{0:T(128)S(1)} %fusion.30, f32[32,64,256]{2,1,0:T(8,128)S(1)} %bitcast.94), kind=kCustom, calls=%fused_computation.5 | custom fusion | bytes 6291584 | tf_op jit(solution)/shard_map/scatter | solution.py:111
  196.2 4.2 convolution_convert_fusion.4
  200.5 63.5 %all-to-all-done.2 = f32[16,4,64,256]{3,2,1,0:T(8,128)} async-done(((f32[16,4,64,256]{3,2,1,0:T(8,128)}), f32[16,4,64,256]{3,2,1,0:T(8,128)}, u32[]{:S(2)}, u32[]{:S(2)}) %all-to-all-start.2) | async-done | bytes 4194336 | tf_op jit(solution)/shard_map/all_to_all | solution.py:114
  264.0 19.2 %all-to-all-start.3 = ((f32[16,4,64,256]{3,2,1,0:T(8,128)}), f32[16,4,64,256]{3,2,1,0:T(8,128)}, u32[]{:S(2)}, u32[]{:S(2)}) async-start(f32[16,4,64,256]{3,2,1,0:T(8,128)} %bitcast.87), calls=%async_computation.4 | async-start | bytes 8388608 | tf_op jit(solution)/shard_map/all_to_all | solution.py:121
  283.3 0.7 fusion.37
  284.0 0.4 copy-done.4
  284.5 2.8 convolution_add_fusion.1
  287.7 6.5 %copy.49 = f32[8,8,64,256]{3,1,2,0:T(8,128)} copy(f32[8,8,64,256]{3,2,1,0:T(8,128)} %bitcast.42) | data formatting | bytes 8388608
  294.3 67.3 %all-to-all-done.3 = f32[16,4,64,256]{3,2,1,0:T(8,128)} async-done(((f32[16,4,64,256]{3,2,1,0:T(8,128)}), f32[16,4,64,256]{3,2,1,0:T(8,128)}, u32[]{:S(2)}, u32[]{:S(2)}) %all-to-all-start.3) | async-done | bytes 4194336 | tf_op jit(solution)/shard_map/all_to_all | solution.py:121
  361.6 4.6 copy.50
  366.1 1.6 convolution_convert_fusion
  367.8 0.5 reshape_reshape.8
  368.3 7.0 %convolution_bitcast_fusion = f32[2048,256]{0,1:T(8,128)} fusion(bf16[2048,256]{1,0:T(8,128)(2,1)S(1)} %reshape_reshape.8, bf16[2048,2048]{1,0:T(8,128)(2,1)} %bitcast.91), kind=kOutput, calls=%fused_computation.12 | convolution fusion | flops 2147483648 | bytes 11534336 | tf_op jit(solution)/shard_map/dot_general | solution.py:147
  375.4 0.3 reduce-scatter.5.cloned.1.call-start
  375.6 3.8 convolution_convert_fusion.1
  379.4 0.5 reshape_reshape.7
  380.0 3.6 fusion.38
  383.6 9.7 %convolution_add_fusion = f32[2048,2048]{1,0:T(8,128)} fusion(f32[2048,2048]{1,0:T(8,128)S(1)} %fusion.38, bf16[2048,256]{1,0:T(8,128)(2,1)S(1)} %reshape_reshape.8, bf16[2048,256]{1,0:T(8,128)(2,1)} %param.14), kind=kOutput, calls=%fused_computation.10 | convolution fusion | flops 2151677952 | bytes 35651584 | tf_op jit(solution)/shard_map/dot_general | solution.py:169
  393.4 3.0 convert_element_type.63
  396.4 118.7 %all-reduce.2.cloned.1.call-done = f32[2048,256]{0,1:T(8,128)} async-done(((f32[2048,256]{0,1:T(8,128)}), f32[2048,256]{0,1:T(8,128)}) %all-reduce.2.cloned.1.call-update) | async-done | bytes 2097168 | tf_op jit(solution)/shard_map/psum | solution.py:153
  515.1 3.0 copy.48
  518.1 6.0 %convert_element_type.66 = bf16[16,64,2048]{2,1,0:T(8,128)(2,1)} convert(f32[16,64,2048]{2,1,0:T(8,128)} %reduce-scatter.5.cloned.1.call-done) | non-fusion elementwise | flops 2097152 | bytes 12582912 | tf_op jit(solution)/shard_map/convert_element_type | solution.py:177
  (38 shorter events, 1.0 us)
Async XLA Ops:
  8.0 102.7 %copy-start = (bf16[512,2048]{1,0:T(8,128)(2,1)S(1)}, bf16[512,2048]{1,0:T(8,128)(2,1)}, u32[]{:S(2)}) copy-start(bf16[512,2048]{1,0:T(8,128)(2,1)} %param.8) | copy-start | bytes 6291460
  60.0 43.1 %all-to-all-start.1 = ((bf16[16,4,64,256]{3,2,1,0:T(8,128)(2,1)}), bf16[16,4,64,256]{3,2,1,0:T(8,128)(2,1)}, u32[]{:S(2)}, u32[]{:S(2)}) async-start(bf16[16,4,64,256]{3,2,1,0:T(8,128)(2,1)} %bitcast.96), calls=%async_computation.1 | async-start | bytes 4194304 | tf_op jit(solution)/shard_map/all_to_all | solution.py:61
  72.4 38.3 %copy-start.5 = (bf16[2048,256]{1,0:T(8,128)(2,1)S(1)}, bf16[2048,256]{1,0:T(8,128)(2,1)}, u32[]{:S(2)}) copy-start(bf16[2048,256]{1,0:T(8,128)(2,1)} %param.11) | copy-start | bytes 3145732
  103.1 48.0 %all-to-all-start = ((bf16[16,4,64,256]{3,2,1,0:T(8,128)(2,1)}), bf16[16,4,64,256]{3,2,1,0:T(8,128)(2,1)}, u32[]{:S(2)}, u32[]{:S(2)}) async-start(bf16[16,4,64,256]{3,2,1,0:T(8,128)(2,1)} %bitcast.95), calls=%async_computation | async-start | bytes 4194304 | tf_op jit(solution)/shard_map/all_to_all | solution.py:60
  111.4 44.1 %copy-start.8 = (bf16[512,256]{1,0:T(8,128)(2,1)}, bf16[512,256]{1,0:T(8,128)(2,1)S(1)}, u32[]{:S(2)}) copy-start(bf16[512,256]{1,0:T(8,128)(2,1)S(1)} %convolution_convert_fusion.5) | copy-start | bytes 786436
  153.7 0.8 copy-start.3
  158.8 3.1 copy-start.2
  175.9 88.1 %all-to-all-start.2 = ((f32[16,4,64,256]{3,2,1,0:T(8,128)}), f32[16,4,64,256]{3,2,1,0:T(8,128)}, u32[]{:S(2)}, u32[]{:S(2)}) async-start(f32[16,4,64,256]{3,2,1,0:T(8,128)} %bitcast.88), calls=%async_computation.3 | async-start | bytes 8388608 | tf_op jit(solution)/shard_map/all_to_all | solution.py:114
  264.0 19.3 %copy-start.6 = (bf16[2048,256]{1,0:T(8,128)(2,1)S(1)}, bf16[2048,256]{1,0:T(8,128)(2,1)}, u32[]{:S(2)}) copy-start(bf16[2048,256]{1,0:T(8,128)(2,1)} %param.11) | copy-start | bytes 3145732
  264.0 97.6 %all-to-all-start.3 = ((f32[16,4,64,256]{3,2,1,0:T(8,128)}), f32[16,4,64,256]{3,2,1,0:T(8,128)}, u32[]{:S(2)}, u32[]{:S(2)}) async-start(f32[16,4,64,256]{3,2,1,0:T(8,128)} %bitcast.87), calls=%async_computation.4 | async-start | bytes 8388608 | tf_op jit(solution)/shard_map/all_to_all | solution.py:121
  283.2 1.2 copy-start.4
  283.2 1.3 copy-start.7
  283.2 110.1 %reduce-scatter.3.cloned.1.call-start = ((), (), s32[]{:S(2)}) async-start(), calls=%async_computation.6 | async-start | bytes 6291456 | tf_op jit(solution)/shard_map/reduce_scatter | solution.py:154
  287.4 227.7 %all-reduce.2.cloned.1.call-start = ((), (), s32[]{:S(2)}) async-start(), calls=%async_computation.8 | async-start | bytes 4194304 | tf_op jit(solution)/shard_map/psum | solution.py:153
  375.4 142.7 %reduce-scatter.5.cloned.1.call-start = ((), (), s32[]{:S(2)}) async-start(), calls=%async_computation.7 | async-start | bytes 25165824 | tf_op jit(solution)/shard_map/reduce_scatter | solution.py:170
  515.1 9.1 %copy-start.1 = (bf16[512,2048]{1,0:T(8,128)(2,1)S(1)}, bf16[512,2048]{1,0:T(8,128)(2,1)}, u32[]{:S(2)}) copy-start(bf16[512,2048]{1,0:T(8,128)(2,1)} %param.8) | copy-start | bytes 6291460
Sparse Core Ops, SparseCore 0:
  287.5 13.2 reduce-scatter.2
  393.5 38.9 reduce-scatter.4
Sparse Core Ops, SparseCore 1:
  375.5 139.5 all-reduce.1
where the time goes:
time: 533 us; the launch traced here: 532 us
  waiting for transfers between devices  317 us (59%)
  matrix products  61.7 us (12%)
  blocking collectives  42.9 us (8%)
  local copies, waits for them, and re-layouts  42.3 us (8%)
  starting transfers between devices  41.4 us (8%)
  between operations  15.7 us (3%)
  other arithmetic  10.9 us (2%)
    psum x1, waiting for transfers between devices, body(): grad_value_weight = lax.psum(weight_part, 'st')  119 us
    all_to_all x1, waiting for transfers between devices, body(): lax.all_to_all(back_values.reshape(owner_count, capacity, span_rows, loca...  67.3 us
    all_to_all x1, waiting for transfers between devices, body(): lax.all_to_all(back_keys.reshape(owner_count, capacity, span_rows, local_...  63.5 us
    all_gather x1, blocking collectives, body(): lax.all_gather(passage_ids, 'st', axis=0, tiled=True)  42.9 us
    all_to_all x1, waiting for transfers between devices, body(): lax.all_to_all(keys_here[slot_table], 'st', split_axis=0, concat_axis=0,...  36.4 us
    all_to_all x1, waiting for transfers between devices, body(): lax.all_to_all(values_here[slot_table], 'st', split_axis=0, concat_axis=0...  30.7 us
    all_to_all x1, starting transfers between devices, body(): lax.all_to_all(back_values.reshape(owner_count, capacity, span_rows, loca...  19.2 us
    unnamed x21, local copies, waits for them, and re-layouts  15.4 us
  transfers between devices with their start and end apart: 7, of which 5 were waited for; matrix products, arithmetic and copies ran while one was open for 14% of the time, Pallas kernels for 0%

commit v1 on v0

v1 whole, which is shorter than its diff:
```python
import functools

import jax
import jax.numpy as jnp
from jax import lax
from jax.experimental import pallas as pl
from jax.experimental.pallas import tpu as pltpu
from jax.sharding import PartitionSpec as P

HEAD_DIM = 256
NT = (((1,), (1,)), ((), ()))
TN = (((0,), (0,)), ((), ()))


def attend_kernel(per_block, span, heads, flat_ref, q_ref, gate_ref, up_ref, da_ref, k_ref, v_ref, dq_ref, dg_ref, out_ref):
    b = pl.program_id(0)

    @pl.when(b == 0)
    def _():
        out_ref[...] = jnp.zeros_like(out_ref)

    score_scale = HEAD_DIM ** (-0.5)
    slots = [flat_ref[b * per_block + j] for j in range(per_block)]
    keys = jnp.concatenate([k_ref[s] for s in slots], axis=0)
    values = jnp.concatenate([v_ref[s] for s in slots], axis=0)
    for h in range(heads):
        cols = slice(h * HEAD_DIM, (h + 1) * HEAD_DIM)
        k, v = keys[:, cols], values[:, cols]
        q, da = q_ref[:, cols], da_ref[:, cols]
        scores = lax.dot_general(q, k, NT, preferred_element_type=jnp.float32) * score_scale
        top = jnp.max(scores, axis=-1, keepdims=True)
        e = jnp.exp(scores - top)
        probs = e / jnp.sum(e, axis=-1, keepdims=True)
        attended = jnp.dot(probs.astype(jnp.bfloat16), v, preferred_element_type=jnp.float32)
        gates = gate_ref[:, cols]
        s = jax.nn.sigmoid(gates)
        up = up_ref[:, cols].astype(jnp.float32)
        dg_ref[:, cols] = (up * attended * s * (1.0 + gates * (1.0 - s))).astype(jnp.bfloat16)
        d_probs = lax.dot_general(da, v, NT, preferred_element_type=jnp.float32)
        centre = jnp.sum(probs * d_probs, axis=-1, keepdims=True)
        d_scores = probs * (d_probs - centre) * score_scale
        dq_ref[:, cols] = jnp.dot(
            d_scores.astype(jnp.bfloat16), k, preferred_element_type=jnp.float32
        ).astype(jnp.bfloat16)
        for j, slot in enumerate(slots):
            rows = slice(j * span, (j + 1) * span)
            out_ref[slot, :, h * 2 * span : (h + 1) * 2 * span] = jnp.concatenate(
                [probs[:, rows], d_scores[:, rows]], axis=1
            ).astype(jnp.bfloat16)


def totals_kernel(unroll, heads, held, span, passage_ref, row_ref, pd_ref, *rest):
    del row_ref
    g_refs = rest[:unroll]
    kt_ref, vt_ref, acc_k, acc_v = rest[unroll:]
    step = pl.program_id(0)
    width = heads * HEAD_DIM

    @pl.when(step == 0)
    def _():
        acc_k[...] = jnp.zeros_like(acc_k)
        acc_v[...] = jnp.zeros_like(acc_v)

    for u in range(unroll):
        p = passage_ref[step * unroll + u]
        for h in range(heads):
            cols = slice(h * HEAD_DIM, (h + 1) * HEAD_DIM)
            a = pd_ref[u, :, h * 2 * span : (h + 1) * 2 * span]
            both = jnp.concatenate(
                [g_refs[u][0, :, cols], g_refs[u][0, :, width + h * HEAD_DIM : width + (h + 1) * HEAD_DIM]],
                axis=1,
            )
            r = lax.dot_general(a, both, TN, preferred_element_type=jnp.float32)
            acc_v[p, :, cols] += r[:span, HEAD_DIM:]
            acc_k[p, :, cols] += r[span:, :HEAD_DIM]

    @pl.when(step == pl.num_programs(0) - 1)
    def _():
        kt_ref[...] = acc_k[:held].astype(jnp.bfloat16)
        vt_ref[...] = acc_v[:held].astype(jnp.bfloat16)


def body(
    hidden,
    passage_store,
    passage_ids,
    query_weight,
    gate_weight,
    key_weight,
    value_weight,
    output_grad,
):
    owner_count = lax.axis_size("st")
    tp_count = lax.axis_size("tp")
    tp_index = lax.axis_index("tp")
    held, span, model_width = passage_store.shape
    block_count, per_block = passage_ids.shape
    requests = block_count * per_block
    capacity = max(1, 2 * requests // owner_count)
    slot_total = owner_count * capacity
    width = query_weight.shape[1]
    heads = width // HEAD_DIM
    tokens = hidden.shape[0]
    block_rows = tokens // block_count
    bf16, f32 = jnp.bfloat16, jnp.float32
    exchange = [(i, tp_count - 1 - i) for i in range(tp_count)]

    ids = passage_ids.reshape(requests)
    owner_of = ids // held
    local_index = ids % held
    positions = jnp.arange(requests, dtype=jnp.int32)
    earlier = positions[None, :] < positions[:, None]
    rank = jnp.sum((owner_of[:, None] == owner_of[None, :]) & earlier, axis=1, dtype=jnp.int32)
    slot_flat = owner_of * capacity + rank
    code = local_index * block_count + positions // per_block + 1
    hit = slot_flat[:, None] == jnp.arange(slot_total, dtype=jnp.int32)[None, :]
    table = jnp.sum(jnp.where(hit, code[:, None], 0), axis=0, dtype=jnp.int32)
    came = lax.all_to_all(
        table.reshape(owner_count, capacity), "st", split_axis=0, concat_axis=0, tiled=True
    ).reshape(slot_total)
    filled = came > 0
    came0 = jnp.maximum(came - 1, 0)
    slot_passage = came0 // block_count
    slot_target = jnp.where(filled, slot_passage, held).astype(jnp.int32)
    reader = jnp.arange(slot_total, dtype=jnp.int32) // capacity
    slot_row = (reader * block_count + came0 % block_count).astype(jnp.int32)

    store_rows = passage_store.reshape(held * span, model_width)

    def project(rows, weight):
        return jnp.dot(rows, weight, preferred_element_type=f32)

    keys_here = project(store_rows, key_weight).astype(bf16).reshape(held, span, width)
    values_here = project(store_rows, value_weight).astype(bf16).reshape(held, span, width)
    came_keys = lax.all_to_all(
        keys_here[slot_passage].reshape(owner_count, capacity, span, width),
        "st", split_axis=0, concat_axis=0, tiled=True,
    ).reshape(slot_total, span, width)
    came_values = lax.all_to_all(
        values_here[slot_passage].reshape(owner_count, capacity, span, width),
        "st", split_axis=0, concat_axis=0, tiled=True,
    ).reshape(slot_total, span, width)

    queries = project(hidden, query_weight).astype(bf16)
    gates = project(hidden, gate_weight)
    d_attended = (output_grad.astype(f32) * gates * jax.nn.sigmoid(gates)).astype(bf16)
    shared = lax.all_gather(
        jnp.concatenate([queries, d_attended], axis=1), "st", axis=0, tiled=True
    ).reshape(owner_count * block_count, block_rows, 2 * width)

    token_weight = jnp.concatenate([query_weight, gate_weight], axis=1)
    token_weight = jnp.concatenate(
        [token_weight, lax.ppermute(token_weight, "tp", exchange)], axis=1
    )
    row_weight = jnp.concatenate([key_weight, value_weight], axis=1)
    row_weight = jnp.concatenate([row_weight, lax.ppermute(row_weight, "tp", exchange)], axis=1)

    whole3 = lambda b, f: (0, 0, 0)
    by_block = pl.BlockSpec((block_rows, width), lambda b, f: (b, 0))
    d_queries, d_gates, pair_slots = pl.pallas_call(
        functools.partial(attend_kernel, per_block, span, heads),
        grid_spec=pltpu.PrefetchScalarGridSpec(
            num_scalar_prefetch=1,
            grid=(block_count,),
            in_specs=[by_block] * 4 + [pl.BlockSpec((slot_total, span, width), whole3)] * 2,
            out_specs=[
                by_block,
                by_block,
                pl.BlockSpec((slot_total, block_rows, heads * 2 * span), whole3),
            ],
        ),
        out_shape=[
            jax.ShapeDtypeStruct((tokens, width), bf16),
            jax.ShapeDtypeStruct((tokens, width), bf16),
            jax.ShapeDtypeStruct((slot_total, block_rows, heads * 2 * span), bf16),
        ],
        cost_estimate=pl.CostEstimate(flops=2_000_000_000, bytes_accessed=8_000_000, transcendentals=0),
        name="attend",
    )(slot_flat, queries, gates, output_grad, d_attended, came_keys, came_values)

    came_pairs = lax.all_to_all(
        pair_slots.reshape(owner_count, capacity, block_rows, heads * 2 * span),
        "st", split_axis=0, concat_axis=0, tiled=True,
    ).reshape(slot_total, block_rows, heads * 2 * span)

    unroll = 4 if slot_total % 4 == 0 else 1

    def shared_spec(u):
        return pl.BlockSpec(
            (1, block_rows, 2 * width), lambda i, p, r: (r[i * unroll + u], 0, 0)
        )

    key_low, value_low = pl.pallas_call(
        functools.partial(totals_kernel, unroll, heads, held, span),
        grid_spec=pltpu.PrefetchScalarGridSpec(
            num_scalar_prefetch=2,
            grid=(slot_total // unroll,),
            in_specs=[
                pl.BlockSpec((unroll, block_rows, heads * 2 * span), lambda i, p, r: (i, 0, 0))
            ]
            + [shared_spec(u) for u in range(unroll)],
            out_specs=[pl.BlockSpec((held, span, width), lambda i, p, r: (0, 0, 0))] * 2,
            scratch_shapes=[pltpu.VMEM((held + 1, span, width), f32)] * 2,
        ),
        out_shape=[jax.ShapeDtypeStruct((held, span, width), bf16)] * 2,
        cost_estimate=pl.CostEstimate(flops=2_000_000_000, bytes_accessed=8_000_000, transcendentals=0),
        name="totals",
    )(slot_target, slot_row, came_pairs, *([shared] * unroll))

    def over_heads(first, second, weight):
        rows = jnp.concatenate([first, second], axis=1)
        half = rows.shape[0] // tp_count
        theirs = lax.dynamic_slice_in_dim(rows, (tp_count - 1 - tp_index) * half, half, 0)
        mine = lax.dynamic_slice_in_dim(rows, tp_index * half, half, 0)
        got = lax.ppermute(theirs, "tp", exchange)
        both = jnp.concatenate([mine, got], axis=1)
        return lax.dot_general(both, weight, NT, preferred_element_type=f32).astype(bf16)

    grad_hidden = over_heads(d_queries, d_gates, token_weight)

    value_rows = value_low.reshape(held * span, width)
    weight_part = lax.dot_general(store_rows, value_rows, TN, preferred_element_type=f32)
    parts = lax.all_to_all(
        weight_part.astype(bf16).reshape(owner_count, model_width // owner_count, width),
        "st", split_axis=0, concat_axis=0, tiled=True,
    )
    weight_sum = jnp.sum(parts.astype(f32), axis=0)
    grad_value_weight = lax.all_gather(weight_sum, "st", axis=0, tiled=True)

    grad_store = over_heads(key_low.reshape(held * span, width), value_rows, row_weight).reshape(
        held // tp_count, span, model_width
    )
    return (grad_hidden, grad_store, grad_value_weight)


def solution(mesh):
    placed = (
        P("st", None),
        P("st", None, None),
        P("st", None),
        P(None, "tp"),
        P(None, "tp"),
        P(None, "tp"),
        P(None, "tp"),
        P("st", "tp"),
    )
    return jax.shard_map(
        body,
        mesh=mesh,
        in_specs=placed,
        out_specs=(P(("st", "tp"), None), P(("st", "tp"), None, None), P(None, "tp")),
        check_vma=False,
    )
```

time: 533 us -> 367 us (0.69)
  waiting for transfers between devices: 317 us -> 122 us
  blocking collectives: 42.9 us -> 127 us
  local copies, waits for them, and re-layouts: 42.3 us -> 13 us
  matrix products: 61.7 us -> 34.5 us
  Pallas kernels: 0 us -> 24.6 us
  starting transfers between devices: 41.4 us -> 20.4 us
    all_to_all x0 -> x2, blocking collectives: none -> 127 us  [the longest x1 96.3 us: body(): lax.all_to_all(values_here[slot_passage].reshape(owner_count, capacity, s...]
    psum x1 -> x0, waiting for transfers between devices: 119 us -> none  [body(): grad_value_weight = lax.psum(weight_part, 'st')]
    all_to_all x4 -> x3, waiting for transfers between devices: 198 us -> 80.5 us  [the longest x1 57 us: body(): lax.all_to_all(keys_here[slot_passage].reshape(owner_count, capacity, spa...]
    all_gather x1 -> x0, blocking collectives: 42.9 us -> none  [body(): lax.all_gather(passage_ids, 'st', axis=0, tiled=True)]
    all_gather x0 -> x2, waiting for transfers between devices: none -> 38.5 us  [the longest x1 38.5 us: body(): grad_value_weight = lax.all_gather(weight_sum, 'st', axis=0, tiled=True)]
    dot_general x17 -> x7, matrix products: 61.7 us -> 34.5 us  [the longest x4 15.9 us: project(): return jnp.dot(rows, weight, preferred_element_type=f32)]
    pallas_call x0 -> x2, Pallas kernels: none -> 24.6 us  [the longest x1 13.9 us: body(): pl.pallas_call(functools.partial(totals_kernel, unroll, heads, held, span...]
    all_to_all x4 -> x3, starting transfers between devices: 41.1 us -> 19.3 us  [the longest x1 8.34 us: body(): lax.all_to_all(table.reshape(owner_count, capacity), 'st', split_axis=0,...]
  transfers between devices with their start and end apart: 7 -> 9, of which waited for: 5 -> 5; matrix products, arithmetic and copies ran while one was open for 14% -> 11% of each run, Pallas kernels for 0% -> 3%
where the time goes in v1:
time: 367 us; the launch traced here: 365 us
  blocking collectives  127 us (35%)
  waiting for transfers between devices  122 us (33%)
  matrix products  34.5 us (9%)
  Pallas kernels  24.6 us (7%)
  starting transfers between devices  20.4 us (6%)
  between operations  14.3 us (4%)
  local copies, waits for them, and re-layouts  13 us (4%)
  other arithmetic  9.82 us (3%)
    all_to_all x1, blocking collectives, body(): lax.all_to_all(values_here[slot_passage].reshape(owner_count, capacity, s...  96.3 us
    all_to_all x1, waiting for transfers between devices, body(): lax.all_to_all(keys_here[slot_passage].reshape(owner_count, capacity, spa...  57 us
    all_gather x1, waiting for transfers between devices, body(): grad_value_weight = lax.all_gather(weight_sum, 'st', axis=0, tiled=True)  38.5 us
    all_to_all x1, blocking collectives, body(): lax.all_to_all(weight_part.astype(bf16).reshape(owner_count, model_width...  30.7 us
    all_to_all x1, waiting for transfers between devices, body(): lax.all_to_all(pair_slots.reshape(owner_count, capacity, block_rows, head...  22.8 us
    dot_general x4, matrix products, project(): return jnp.dot(rows, weight, preferred_element_type=f32)  15.9 us
    pallas_call x1, Pallas kernels, body(): pl.pallas_call(functools.partial(totals_kernel, unroll, heads, held, span...  13.9 us
    dot_general x2, matrix products, over_heads(): lax.dot_general(both, weight, NT, preferred_element_type=f32).astype(bf16)  12.5 us
  transfers between devices with their start and end apart: 9, of which 5 were waited for; matrix products, arithmetic and copies ran while one was open for 11% of the time, Pallas kernels for 3%

profile of v1, /device:TPU:0, one launch (start us, length us, event | category | flops | bytes accessed | tf_op | source)
XLA Modules:
  0.0 365.3 jit_solution(2375838355706976807)
XLA Ops:
  7.2 1.5 copy-done
  8.8 2.0 convolution_convert_fusion.2.q_ref
  10.8 1.5 multiply_convert_fusion
  12.3 0.7 copy-done.14
  13.0 0.9 pad_maximum_fusion.2
  13.9 0.1 copy.30
  14.0 0.1 reshape.236
  14.1 0.2 convert_reduce_fusion.1
  14.3 0.1 select_reduce_fusion
  14.4 0.7 all_to_all.18
  15.1 8.3 %all-to-all-start = ((s32[16,1,4]{2,1,0:T(1,128)}), s32[16,1,4]{2,1,0:T(1,128)S(1)}, u32[]{:S(2)}, u32[]{:S(2)}) async-start(s32[16,1,4]{2,1,0:T(1,128)} %bitcast.2), calls=%async_computation | async-start | bytes 16384 | tf_op jit(solution)/shard_map/all_to_all | solution.py:118
  23.5 6.5 %convolution_convert_fusion.1 = bf16[2048,256]{1,0:T(8,128)(2,1)S(1)} fusion(bf16[2048,2048]{1,0:T(8,128)(2,1)} %bitcast.43, bf16[2048,256]{1,0:T(8,128)(2,1)} %param.13), kind=kOutput, calls=%fused_computation.19 | convolution fusion | flops 2148007936 | bytes 10485760 | tf_op jit(solution)/shard_map/dot_general | solution.py:131
  30.0 0.7 all-to-all-done
  30.7 0.1 and_reduce_fusion.1
  30.7 0.1 div.50
  30.8 0.1 compare_reduce_fusion.1
  30.9 0.1 reshape.251
  31.1 2.0 gather_fusion
  33.1 6.2 %all-to-all-start.1 = ((bf16[16,4,64,256]{3,2,1,0:T(8,128)(2,1)}), bf16[16,4,64,256]{3,2,1,0:T(8,128)(2,1)}, u32[]{:S(2)}, u32[]{:S(2)}) async-start(bf16[16,4,64,256]{3,2,1,0:T(8,128)(2,1)} %bitcast.45), calls=%async_computation.1 | async-start | bytes 4194304 | tf_op jit(solution)/shard_map/all_to_all | solution.py:135
  39.3 6.0 %convolution_convert_fusion = bf16[2048,256]{1,0:T(8,128)(2,1)S(1)} fusion(bf16[2048,2048]{1,0:T(8,128)(2,1)} %bitcast.44, bf16[2048,256]{1,0:T(8,128)(2,1)} %param.14), kind=kOutput, calls=%fused_computation.18 | convolution fusion | flops 2148007936 | bytes 10485760 | tf_op jit(solution)/shard_map/dot_general | solution.py:131
  45.3 2.0 gather_fusion.1
  47.3 57.0 %all-to-all-done.1 = bf16[16,4,64,256]{3,2,1,0:T(8,128)(2,1)} async-done(((bf16[16,4,64,256]{3,2,1,0:T(8,128)(2,1)}), bf16[16,4,64,256]{3,2,1,0:T(8,128)(2,1)}, u32[]{:S(2)}, u32[]{:S(2)}) %all-to-all-start.1) | async-done | bytes 2097184 | tf_op jit(solution)/shard_map/all_to_all | solution.py:135
  104.3 96.3 %all_to_all.29 = bf16[16,4,64,256]{3,2,1,0:T(8,128)(2,1)} all-to-all(bf16[16,4,64,256]{3,2,1,0:T(8,128)(2,1)} %bitcast.46), channel_id=1, replica_groups=mesh['st'=16,'tp'=2] {'st'}, dimensions={0} | all-to-all | bytes 4194304 | tf_op jit(solution)/shard_map/all_to_all | solution.py:139
  200.6 10.7 %attend.1 = (bf16[512,256]{1,0:T(8,128)(2,1)}, bf16[512,256]{1,0:T(8,128)(2,1)}, bf16[64,64,128]{2,1,0:T(8,128)(2,1)}) custom-call(s32[32]{0:T(128)} %copy-done.17, bf16[512,256]{1,0:T(8,128)(2,1)} %copy-done.13, f32[512,256]{1,0:T(8,128)} %get-tuple-element.34.gate_ref, bf16[512,256]{1,0:T(8,128)(2,1)} %up_ref.1, bf16[512,256]{1,0:T(8,128)(2,1)} %copy-done.14, ...), custom_call_target="tpu_custom_call" | custom-call | flops 2000000000 | bytes 8000000 | tf_op jit(solution)/shard_map/attend/pallas_call | solution.py:160
  211.3 4.7 %all-to-all-start.3 = ((bf16[16,4,64,128]{3,2,1,0:T(8,128)(2,1)}), bf16[16,4,64,128]{3,2,1,0:T(8,128)(2,1)S(1)}, u32[]{:S(2)}, u32[]{:S(2)}) async-start(bf16[16,4,64,128]{3,2,1,0:T(8,128)(2,1)} %bitcast.54), calls=%async_computation.3 | async-start | bytes 2097152 | tf_op jit(solution)/shard_map/all_to_all | solution.py:181
  216.0 0.1 div.51
  216.1 0.1 rem.63
  216.2 0.1 gt.7
  216.3 0.1 ne.131
  216.4 0.5 fusion.29
  216.9 22.8 %all-to-all-done.3 = bf16[16,4,64,128]{3,2,1,0:T(8,128)(2,1)S(1)} async-done(((bf16[16,4,64,128]{3,2,1,0:T(8,128)(2,1)}), bf16[16,4,64,128]{3,2,1,0:T(8,128)(2,1)S(1)}, u32[]{:S(2)}, u32[]{:S(2)}) %all-to-all-start.3) | async-done | bytes 1048608 | tf_op jit(solution)/shard_map/all_to_all | solution.py:181
  239.7 1.0 copy-done.2
  240.7 13.9 %totals.1 = (bf16[32,64,256]{2,1,0:T(8,128)(2,1)}, bf16[32,64,256]{2,1,0:T(8,128)(2,1)}) custom-call(s32[64]{0:T(128)} %get-tuple-element.30.passage_ref, s32[64]{0:T(128)} %get-tuple-element.29.row_ref, bf16[64,64,128]{2,1,0:T(8,128)(2,1)} %bitcast.48, bf16[128,64,512]{2,1,0:T(8,128)(2,1)} %bitcast.39, bf16[128,64,512]{2,1,0:T(8,128)(2,1)} %bitcast.40, ...), custom_call_target="tpu_custom_call" | custom-call | flops 2000000000 | bytes 8000000 | tf_op jit(solution)/shard_map/totals/pallas_call | solution.py:193
  254.6 6.1 %fusion.22 = bf16[32,16,8,128]{3,2,1,0:T(8,128)(2,1)S(1)} fusion(bf16[32,64,256]{2,1,0:T(8,128)(2,1)} %get-tuple-element.12, bf16[32,64,2048]{2,1,0:T(8,128)(2,1)} %param.9), kind=kOutput, calls=%fused_computation.30 | convolution fusion | flops 2148007936 | bytes 10485760 | tf_op jit(solution)/shard_map/dot_general | solution.py:222
  260.7 0.3 copy.44
  261.0 30.7 %all_to_all.30 = bf16[16,128,256]{1,2,0:T(8,128)(2,1)S(1)} all-to-all(bf16[16,128,256]{1,2,0:T(8,128)(2,1)S(1)} %bitcast.51), channel_id=1, replica_groups=mesh['st'=16,'tp'=2] {'st'}, dimensions={0} | all-to-all | bytes 2097152 | tf_op jit(solution)/shard_map/all_to_all | solution.py:223
  291.6 0.8 convert_reduce_fusion
  292.5 2.9 pad_maximum_fusion
  295.4 1.5 pad_maximum_fusion.1
  296.8 0.5 collective-permute-start.3
  297.3 2.8 fusion.24
  300.2 1.1 constant_dynamic-update-slice_fusion.1
  301.4 0.5 collective-permute-start
  301.9 2.7 collective-permute-done
  304.6 4.0 %fusion.15 = bf16[256,2048]{1,0:T(8,128)(2,1)} fusion(bf16[2048,512]{1,0:T(8,128)(2,1)} %collective-permute-done.1, bf16[2048,256]{1,0:T(8,128)(2,1)S(1)} %copy-done.6, bf16[2048,256]{1,0:T(8,128)(2,1)S(1)} %copy-done.7, bf16[256,512]{1,0:T(8,128)(2,1)S(1)} %collective-permute-done, bf16[256,512]{1,0:T(8,128)(2,1)S(1)} %get-tuple-element.26), kind=kOutput, calls=%fused_computation.16 | convolution fusion | flops 1087897600 | bytes 5767168 | tf_op jit(solution)/shard_map/dot_general | solution.py:217
  308.7 8.5 %fusion.12 = bf16[1024,2048]{1,0:T(8,128)(2,1)} fusion(bf16[2048,512]{1,0:T(8,128)(2,1)} %collective-permute-done.3, bf16[2048,256]{1,0:T(8,128)(2,1)S(1)} %copy-done.11, bf16[2048,256]{1,0:T(8,128)(2,1)S(1)} %copy-done.9, bf16[1024,512]{1,0:T(8,128)(2,1)} %collective-permute-done.2, bf16[1024,512]{1,0:T(8,128)(2,1)S(1)} %copy-done.3), kind=kOutput, calls=%fused_computation.14 | convolution fusion | flops 4313841664 | bytes 10485760 | tf_op jit(solution)/shard_map/dot_general | solution.py:217
  317.2 38.5 %all-gather.5.cloned.1.call-done = f32[2048,256]{0,1:T(8,128)} async-done(((f32[128,256]{0,1:T(8,128)}), f32[2048,256]{0,1:T(8,128)}) %all-gather.5.cloned.1.call-update) | async-done | bytes 2097168 | tf_op jit(solution)/shard_map/all_gather | solution.py:228
  355.6 2.9 copy.38
  (49 shorter events, 0.3 us)
Async XLA Ops:
  7.2 1.6 copy-start
  7.2 3.6 copy-start.4
  7.2 232.5 %all-gather.3.cloned.1.call-start = ((), (), s32[]{:S(2)}) async-start(), calls=%async_computation.5 | async-start | bytes 8912896 | tf_op jit(solution)/shard_map/all_gather | solution.py:147
  8.8 2.0 copy-start.16
  10.8 1.6 copy-start.13
  10.8 3.2 copy-start.15
  12.3 0.7 copy-start.14
  14.3 15.6 %copy-start.17 = (s32[32]{0:T(128)}, s32[32]{0:T(128)S(1)}, u32[]{:S(2)}) copy-start(s32[32]{0:T(128)S(1)} %multiply_add_fusion.flat_ref) | copy-start | bytes 388
  15.1 15.6 %all-to-all-start = ((s32[16,1,4]{2,1,0:T(1,128)}), s32[16,1,4]{2,1,0:T(1,128)S(1)}, u32[]{:S(2)}, u32[]{:S(2)}) async-start(s32[16,1,4]{2,1,0:T(1,128)} %bitcast.2), calls=%async_computation | async-start | bytes 16384 | tf_op jit(solution)/shard_map/all_to_all | solution.py:118
  33.1 71.2 %all-to-all-start.1 = ((bf16[16,4,64,256]{3,2,1,0:T(8,128)(2,1)}), bf16[16,4,64,256]{3,2,1,0:T(8,128)(2,1)}, u32[]{:S(2)}, u32[]{:S(2)}) async-start(bf16[16,4,64,256]{3,2,1,0:T(8,128)(2,1)} %bitcast.45), calls=%async_computation.1 | async-start | bytes 4194304 | tf_op jit(solution)/shard_map/all_to_all | solution.py:135
  211.3 28.4 %all-to-all-start.3 = ((bf16[16,4,64,128]{3,2,1,0:T(8,128)(2,1)}), bf16[16,4,64,128]{3,2,1,0:T(8,128)(2,1)S(1)}, u32[]{:S(2)}, u32[]{:S(2)}) async-start(bf16[16,4,64,128]{3,2,1,0:T(8,128)(2,1)} %bitcast.54), calls=%async_computation.3 | async-start | bytes 2097152 | tf_op jit(solution)/shard_map/all_to_all | solution.py:181
  216.0 139.6 %all-gather.5.cloned.1.call-start = ((), (), s32[]{:S(2)}) async-start(), calls=%async_computation.6 | async-start | bytes 2228224 | tf_op jit(solution)/shard_map/all_gather | solution.py:228
  239.7 1.0 copy-start.2
  260.9 31.5 %copy-start.5 = (bf16[2048,256]{1,0:T(8,128)(2,1)S(1)}, bf16[2048,256]{1,0:T(8,128)(2,1)}, u32[]{:S(2)}) copy-start(bf16[2048,256]{1,0:T(8,128)(2,1)} %param.12) | copy-start | bytes 3145732
  292.5 2.9 copy-start.8
  292.5 2.9 copy-start.10
  295.3 2.0 copy-start.1
  295.3 6.6 %collective-permute-start.1 = (bf16[2048,512]{1,0:T(8,128)(2,1)}, bf16[2048,512]{1,0:T(8,128)(2,1)}, u32[]{:S(2)}, u32[]{:S(2)}) collective-permute-start(bf16[2048,512]{1,0:T(8,128)(2,1)} %pad_maximum_fusion), channel_id=1, source_target_pairs={{0,1},{1,0},{2,3},{3,2},{4,5},{5,4},{6,7},{7,6},{8,9},{9,8},{10,11... | collective-permute-start | bytes 6291464 | tf_op jit(solution)/shard_map/ppermute | solution.py:153
  296.8 11.8 %collective-permute-start.3 = (bf16[2048,512]{1,0:T(8,128)(2,1)}, bf16[2048,512]{1,0:T(8,128)(2,1)}, u32[]{:S(2)}, u32[]{:S(2)}) collective-permute-start(bf16[2048,512]{1,0:T(8,128)(2,1)} %pad_maximum_fusion.1), channel_id=1, source_target_pairs={{0,1},{1,0},{2,3},{3,2},{4,5},{5,4},{6,7},{7,6},{8,9},{9,8},{10,11... | collective-permute-start | bytes 6291464 | tf_op jit(solution)/shard_map/ppermute | solution.py:156
  297.3 4.0 %copy-start.12 = (bf16[512,256]{1,0:T(8,128)(2,1)S(1)}, bf16[512,256]{1,0:T(8,128)(2,1)}, u32[]{:S(2)}) copy-start(bf16[512,256]{1,0:T(8,128)(2,1)} %get-tuple-element.9) | copy-start | bytes 786436
  300.2 4.4 %copy-start.6 = (bf16[2048,256]{1,0:T(8,128)(2,1)S(1)}, bf16[2048,256]{1,0:T(8,128)(2,1)}, u32[]{:S(2)}) copy-start(bf16[2048,256]{1,0:T(8,128)(2,1)} %param.12) | copy-start | bytes 3145732
  300.2 8.5 %collective-permute-start.2 = (bf16[1024,512]{1,0:T(8,128)(2,1)}, bf16[1024,512]{1,0:T(8,128)(2,1)}, u32[]{:S(2)}, u32[]{:S(2)}) collective-permute-start(bf16[1024,512]{1,0:T(8,128)(2,1)} %get-tuple-element.25), channel_id=1, source_target_pairs={{0,1},{1,0},{2,3},{3,2},{4,5},{5,4},{6,7},{7,6},{8,9},{9,8},{10,11... | collective-permute-start | bytes 3145736 | tf_op jit(solution)/shard_map/ppermute | solution.py:215
  300.2 4.4 %copy-start.7 = (bf16[2048,256]{1,0:T(8,128)(2,1)S(1)}, bf16[2048,256]{1,0:T(8,128)(2,1)}, u32[]{:S(2)}) copy-start(bf16[2048,256]{1,0:T(8,128)(2,1)} %param.11) | copy-start | bytes 3145732
  301.4 3.2 collective-permute-start
  304.6 4.1 %copy-start.3 = (bf16[1024,512]{1,0:T(8,128)(2,1)S(1)}, bf16[1024,512]{1,0:T(8,128)(2,1)}, u32[]{:S(2)}) copy-start(bf16[1024,512]{1,0:T(8,128)(2,1)} %get-tuple-element.24) | copy-start | bytes 3145732
  304.6 4.1 %copy-start.9 = (bf16[2048,256]{1,0:T(8,128)(2,1)S(1)}, bf16[2048,256]{1,0:T(8,128)(2,1)}, u32[]{:S(2)}) copy-start(bf16[2048,256]{1,0:T(8,128)(2,1)} %param.13) | copy-start | bytes 3145732
  304.6 4.1 %copy-start.11 = (bf16[2048,256]{1,0:T(8,128)(2,1)S(1)}, bf16[2048,256]{1,0:T(8,128)(2,1)}, u32[]{:S(2)}) copy-start(bf16[2048,256]{1,0:T(8,128)(2,1)} %param.14) | copy-start | bytes 3145732
Sparse Core Ops, SparseCore 0:
  14.0 184.2 all-gather.2
  292.6 62.9 all-gather.4

commit v2 on v1

v2 whole, which is shorter than its diff:
```python
import functools

import jax
import jax.numpy as jnp
from jax import lax
from jax.experimental import pallas as pl
from jax.experimental.pallas import tpu as pltpu
from jax.sharding import PartitionSpec as P

HEAD_DIM = 256
NT = (((1,), (1,)), ((), ()))
TN = (((0,), (0,)), ((), ()))


def attend_kernel(per_block, span, heads, flat_ref, q_ref, gate_ref, up_ref, da_ref, k_ref, v_ref, dq_ref, dg_ref, dk_ref, dv_ref):
    b = pl.program_id(0)

    @pl.when(b == 0)
    def _():
        dk_ref[...] = jnp.zeros_like(dk_ref)
        dv_ref[...] = jnp.zeros_like(dv_ref)

    score_scale = HEAD_DIM ** (-0.5)
    slots = [flat_ref[b * per_block + j] for j in range(per_block)]
    keys = jnp.concatenate([k_ref[s] for s in slots], axis=0)
    values = jnp.concatenate([v_ref[s] for s in slots], axis=0)
    for h in range(heads):
        cols = slice(h * HEAD_DIM, (h + 1) * HEAD_DIM)
        k, v = keys[:, cols], values[:, cols]
        q, da = q_ref[:, cols], da_ref[:, cols]
        scores = lax.dot_general(q, k, NT, preferred_element_type=jnp.float32) * score_scale
        top = jnp.max(scores, axis=-1, keepdims=True)
        e = jnp.exp(scores - top)
        probs = e / jnp.sum(e, axis=-1, keepdims=True)
        probs_low = probs.astype(jnp.bfloat16)
        attended = jnp.dot(probs_low, v, preferred_element_type=jnp.float32)
        gates = gate_ref[:, cols]
        s = jax.nn.sigmoid(gates)
        up = up_ref[:, cols].astype(jnp.float32)
        dg_ref[:, cols] = (up * attended * s * (1.0 + gates * (1.0 - s))).astype(jnp.bfloat16)
        d_probs = lax.dot_general(da, v, NT, preferred_element_type=jnp.float32)
        centre = jnp.sum(probs * d_probs, axis=-1, keepdims=True)
        d_scores = (probs * (d_probs - centre) * score_scale).astype(jnp.bfloat16)
        dq_ref[:, cols] = jnp.dot(d_scores, k, preferred_element_type=jnp.float32).astype(
            jnp.bfloat16
        )
        d_keys = lax.dot_general(d_scores, q, TN, preferred_element_type=jnp.float32)
        d_values = lax.dot_general(probs_low, da, TN, preferred_element_type=jnp.float32)
        for j, slot in enumerate(slots):
            rows = slice(j * span, (j + 1) * span)
            dk_ref[slot, :, cols] = d_keys[rows].astype(jnp.bfloat16)
            dv_ref[slot, :, cols] = d_values[rows].astype(jnp.bfloat16)


def totals_kernel(unroll, held, passage_ref, came_ref, out_ref, acc):
    step = pl.program_id(0)

    @pl.when(step == 0)
    def _():
        acc[...] = jnp.zeros_like(acc)

    for u in range(unroll):
        acc[passage_ref[step * unroll + u]] += came_ref[u].astype(jnp.float32)

    @pl.when(step == pl.num_programs(0) - 1)
    def _():
        out_ref[...] = acc[:held].astype(jnp.bfloat16)


def body(
    hidden,
    passage_store,
    passage_ids,
    query_weight,
    gate_weight,
    key_weight,
    value_weight,
    output_grad,
):
    owner_count = lax.axis_size("st")
    tp_count = lax.axis_size("tp")
    tp_index = lax.axis_index("tp")
    held, span, model_width = passage_store.shape
    block_count, per_block = passage_ids.shape
    requests = block_count * per_block
    capacity = max(1, 2 * requests // owner_count)
    slot_total = owner_count * capacity
    width = query_weight.shape[1]
    heads = width // HEAD_DIM
    tokens = hidden.shape[0]
    block_rows = tokens // block_count
    bf16, f32 = jnp.bfloat16, jnp.float32
    exchange = [(i, tp_count - 1 - i) for i in range(tp_count)]

    ids = passage_ids.reshape(requests)
    owner_of = ids // held
    local_index = ids % held
    positions = jnp.arange(requests, dtype=jnp.int32)
    earlier = positions[None, :] < positions[:, None]
    rank = jnp.sum((owner_of[:, None] == owner_of[None, :]) & earlier, axis=1, dtype=jnp.int32)
    slot_flat = owner_of * capacity + rank
    code = local_index + 1
    hit = slot_flat[:, None] == jnp.arange(slot_total, dtype=jnp.int32)[None, :]
    table = jnp.sum(jnp.where(hit, code[:, None], 0), axis=0, dtype=jnp.int32)
    came = lax.all_to_all(
        table.reshape(owner_count, capacity), "st", split_axis=0, concat_axis=0, tiled=True
    ).reshape(slot_total)
    filled = came > 0
    slot_passage = jnp.maximum(came - 1, 0)
    slot_target = jnp.where(filled, slot_passage, held).astype(jnp.int32)

    store_rows = passage_store.reshape(held * span, model_width)

    def project(rows, weight):
        return jnp.dot(rows, weight, preferred_element_type=f32)

    keys_here = project(store_rows, key_weight).astype(bf16).reshape(held, span, width)
    values_here = project(store_rows, value_weight).astype(bf16).reshape(held, span, width)
    came_keys = lax.all_to_all(
        keys_here[slot_passage].reshape(owner_count, capacity, span, width),
        "st", split_axis=0, concat_axis=0, tiled=True,
    ).reshape(slot_total, span, width)
    came_values = lax.all_to_all(
        values_here[slot_passage].reshape(owner_count, capacity, span, width),
        "st", split_axis=0, concat_axis=0, tiled=True,
    ).reshape(slot_total, span, width)

    queries = project(hidden, query_weight).astype(bf16)
    gates = project(hidden, gate_weight)
    d_attended = (output_grad.astype(f32) * gates * jax.nn.sigmoid(gates)).astype(bf16)
    token_weight = jnp.concatenate([query_weight, gate_weight], axis=1)
    token_weight = jnp.concatenate(
        [token_weight, lax.ppermute(token_weight, "tp", exchange)], axis=1
    )
    row_weight = jnp.concatenate([key_weight, value_weight], axis=1)
    row_weight = jnp.concatenate([row_weight, lax.ppermute(row_weight, "tp", exchange)], axis=1)

    came_values, token_weight, row_weight = lax.optimization_barrier(
        (came_values, token_weight, row_weight)
    )

    whole3 = lambda b, f: (0, 0, 0)
    by_block = pl.BlockSpec((block_rows, width), lambda b, f: (b, 0))
    d_queries, d_gates, key_slots, value_slots = pl.pallas_call(
        functools.partial(attend_kernel, per_block, span, heads),
        grid_spec=pltpu.PrefetchScalarGridSpec(
            num_scalar_prefetch=1,
            grid=(block_count,),
            in_specs=[by_block] * 4 + [pl.BlockSpec((slot_total, span, width), whole3)] * 2,
            out_specs=[
                by_block,
                by_block,
                pl.BlockSpec((slot_total, span, width), whole3),
                pl.BlockSpec((slot_total, span, width), whole3),
            ],
        ),
        out_shape=[
            jax.ShapeDtypeStruct((tokens, width), bf16),
            jax.ShapeDtypeStruct((tokens, width), bf16),
            jax.ShapeDtypeStruct((slot_total, span, width), bf16),
            jax.ShapeDtypeStruct((slot_total, span, width), bf16),
        ],
        cost_estimate=pl.CostEstimate(flops=2_000_000_000, bytes_accessed=8_000_000, transcendentals=0),
        name="attend",
    )(slot_flat, queries, gates, output_grad, d_attended, came_keys, came_values)

    unroll = 8 if slot_total % 8 == 0 else 1

    def totals(slots):
        came = lax.all_to_all(
            slots.reshape(owner_count, capacity, span, width),
            "st", split_axis=0, concat_axis=0, tiled=True,
        ).reshape(slot_total, span, width)
        return pl.pallas_call(
            functools.partial(totals_kernel, unroll, held),
            grid_spec=pltpu.PrefetchScalarGridSpec(
                num_scalar_prefetch=1,
                grid=(slot_total // unroll,),
                in_specs=[pl.BlockSpec((unroll, span, width), lambda i, p: (i, 0, 0))],
                out_specs=pl.BlockSpec((held, span, width), lambda i, p: (0, 0, 0)),
                scratch_shapes=[pltpu.VMEM((held + 1, span, width), f32)],
            ),
            out_shape=jax.ShapeDtypeStruct((held, span, width), bf16),
            cost_estimate=pl.CostEstimate(
                flops=1_000_000_000, bytes_accessed=4_000_000, transcendentals=0
            ),
            name="totals",
        )(slot_target, came)

    value_low = totals(value_slots)
    key_low = totals(key_slots)

    def over_heads(first, second, weight):
        rows = jnp.concatenate([first, second], axis=1)
        half = rows.shape[0] // tp_count
        theirs = lax.dynamic_slice_in_dim(rows, (tp_count - 1 - tp_index) * half, half, 0)
        mine = lax.dynamic_slice_in_dim(rows, tp_index * half, half, 0)
        got = lax.ppermute(theirs, "tp", exchange)
        both = jnp.concatenate([mine, got], axis=1)
        return lax.dot_general(both, weight, NT, preferred_element_type=f32).astype(bf16)

    grad_hidden = over_heads(d_queries, d_gates, token_weight)

    value_rows = value_low.reshape(held * span, width)
    weight_part = lax.dot_general(store_rows, value_rows, TN, preferred_element_type=f32)
    parts = lax.all_to_all(
        weight_part.astype(bf16).reshape(owner_count, model_width // owner_count, width),
        "st", split_axis=0, concat_axis=0, tiled=True,
    )
    weight_sum = jnp.sum(parts.astype(f32), axis=0)
    shared = jnp.broadcast_to(weight_sum.astype(bf16)[None], parts.shape)
    grad_value_weight = (
        lax.all_to_all(shared, "st", split_axis=0, concat_axis=0, tiled=True)
        .reshape(model_width, width)
        .astype(f32)
    )

    grad_store = over_heads(key_low.reshape(held * span, width), value_rows, row_weight).reshape(
        held // tp_count, span, model_width
    )
    return (grad_hidden, grad_store, grad_value_weight)


def solution(mesh):
    placed = (
        P("st", None),
        P("st", None, None),
        P("st", None),
        P(None, "tp"),
        P(None, "tp"),
        P(None, "tp"),
        P(None, "tp"),
        P("st", "tp"),
    )
    return jax.shard_map(
        body,
        mesh=mesh,
        in_specs=placed,
        out_specs=(P(("st", "tp"), None), P(("st", "tp"), None, None), P(None, "tp")),
        check_vma=False,
    )
```

time: 367 us -> 305 us (0.83)
  blocking collectives: 127 us -> 58.1 us
  starting transfers between devices: 20.4 us -> 44.7 us
  between operations: 14.3 us -> 0.92 us
  local copies, waits for them, and re-layouts: 13 us -> 9.17 us
    all_to_all x2 -> x1, blocking collectives: 127 us -> 58.1 us  [totals(): lax.all_to_all(slots.reshape(owner_count, capacity, span, width), 'st', s...]
    all_to_all x1 -> x4, waiting for transfers between devices: 22.8 us -> 86.7 us  [the longest x1 34.8 us: body(): lax.all_to_all(values_here[slot_passage].reshape(owner_count, capacity, s...]
    all_gather x2 -> x0, waiting for transfers between devices: 38.5 us -> none  [the longest x1 38.5 us: body(): grad_value_weight = lax.all_gather(weight_sum, 'st', axis=0, tiled=True)]
    all_to_all x1, waiting for transfers between devices: 57 us -> 31.5 us  [body(): lax.all_to_all(keys_here[slot_passage].reshape(owner_count, capacity, spa...]
    all_to_all x1 -> x4, starting transfers between devices: 4.68 us -> 25.9 us  [the longest x1 9.82 us: body(): lax.all_to_all(weight_part.astype(bf16).reshape(owner_count, model_width...]
    unnamed x39 -> x28, local copies, waits for them, and re-layouts: 7.35 us -> 1.21 us
    all_to_all x1, starting transfers between devices: 6.24 us -> 10 us  [body(): lax.all_to_all(keys_here[slot_passage].reshape(owner_count, capacity, spa...]
    pallas_call x1 -> x2, Pallas kernels: 13.9 us -> 12.4 us  [totals(): pl.pallas_call(functools.partial(totals_kernel, unroll, held), grid_spec=...]
  transfers between devices with their start and end apart: 9 -> 10, of which waited for: 5 -> 9; matrix products, arithmetic and copies ran while one was open for 11% -> 16% of each run, Pallas kernels for 3% -> 4%
where the time goes in v2:
time: 305 us; the launch traced here: 304 us
  waiting for transfers between devices  122 us (40%)
  blocking collectives  58.1 us (19%)
  starting transfers between devices  44.7 us (15%)
  matrix products  33.1 us (11%)
  Pallas kernels  25.2 us (8%)
  other arithmetic  10.9 us (4%)
  local copies, waits for them, and re-layouts  9.17 us (3%)
    all_to_all x1, blocking collectives, totals(): lax.all_to_all(slots.reshape(owner_count, capacity, span, width), 'st', s...  58.1 us
    all_to_all x1, waiting for transfers between devices, body(): lax.all_to_all(values_here[slot_passage].reshape(owner_count, capacity, s...  34.8 us
    all_to_all x1, waiting for transfers between devices, body(): lax.all_to_all(keys_here[slot_passage].reshape(owner_count, capacity, spa...  31.5 us
    all_to_all x1, waiting for transfers between devices, totals(): lax.all_to_all(slots.reshape(owner_count, capacity, span, width), 'st', s...  28 us
    dot_general x4, matrix products, project(): return jnp.dot(rows, weight, preferred_element_type=f32)  15 us
    all_to_all x1, waiting for transfers between devices, body(): lax.all_to_all(weight_part.astype(bf16).reshape(owner_count, model_width...  14.7 us
    pallas_call x1, Pallas kernels, body(): pl.pallas_call(functools.partial(attend_kernel, per_block, span, heads),...  12.8 us
    pallas_call x2, Pallas kernels, totals(): pl.pallas_call(functools.partial(totals_kernel, unroll, held), grid_spec=...  12.4 us
  transfers between devices with their start and end apart: 10, of which 9 were waited for; matrix products, arithmetic and copies ran while one was open for 16% of the time, Pallas kernels for 4%

profile of v2, /device:TPU:0, one launch (start us, length us, event | category | flops | bytes accessed | tf_op | source)
XLA Modules:
  0.0 304.3 jit_solution(10790967857600902404)
XLA Ops:
  0.6 0.9 copy.18
  1.6 0.1 reshape.181
  1.6 0.2 convert_reduce_fusion
  1.8 0.1 select_reduce_fusion
  1.9 0.7 all_to_all.24
  2.6 8.3 %all-to-all-start = ((s32[16,1,4]{2,1,0:T(1,128)}), s32[16,1,4]{2,1,0:T(1,128)S(1)}, u32[]{:S(2)}, u32[]{:S(2)}) async-start(s32[16,1,4]{2,1,0:T(1,128)} %bitcast.2), calls=%async_computation | async-start | bytes 16384 | tf_op jit(solution)/shard_map/all_to_all | solution.py:105
  11.0 6.0 %convolution_convert_fusion.2 = bf16[2048,256]{1,0:T(8,128)(2,1)S(1)} fusion(bf16[2048,2048]{1,0:T(8,128)(2,1)} %bitcast.42, bf16[2048,256]{1,0:T(8,128)(2,1)} %param.14), kind=kOutput, calls=%fused_computation.8 | convolution fusion | flops 2148007936 | bytes 10485760 | tf_op jit(solution)/shard_map/dot_general | solution.py:115
  17.0 1.2 all-to-all-done
  18.3 0.1 reshape.200
  18.4 2.0 gather_fusion.1
  20.4 5.7 %all-to-all-start.2 = ((bf16[16,4,64,256]{3,2,1,0:T(8,128)(2,1)}), bf16[16,4,64,256]{3,2,1,0:T(8,128)(2,1)}, u32[]{:S(2)}, u32[]{:S(2)}) async-start(bf16[16,4,64,256]{3,2,1,0:T(8,128)(2,1)} %bitcast.45), calls=%async_computation.2 | async-start | bytes 4194304 | tf_op jit(solution)/shard_map/all_to_all | solution.py:123
  26.1 6.0 %convolution_convert_fusion.3 = bf16[2048,256]{1,0:T(8,128)(2,1)S(1)} fusion(bf16[2048,2048]{1,0:T(8,128)(2,1)} %bitcast.43, bf16[2048,256]{1,0:T(8,128)(2,1)} %param.13), kind=kOutput, calls=%fused_computation.9 | convolution fusion | flops 2148007936 | bytes 10485760 | tf_op jit(solution)/shard_map/dot_general | solution.py:115
  32.1 2.0 gather_fusion
  34.1 34.8 %all-to-all-done.2 = bf16[16,4,64,256]{3,2,1,0:T(8,128)(2,1)} async-done(((bf16[16,4,64,256]{3,2,1,0:T(8,128)(2,1)}), bf16[16,4,64,256]{3,2,1,0:T(8,128)(2,1)}, u32[]{:S(2)}, u32[]{:S(2)}) %all-to-all-start.2) | async-done | bytes 2097184 | tf_op jit(solution)/shard_map/all_to_all | solution.py:123
  68.9 10.0 %all-to-all-start.1 = ((bf16[16,4,64,256]{3,2,1,0:T(8,128)(2,1)}), bf16[16,4,64,256]{3,2,1,0:T(8,128)(2,1)}, u32[]{:S(2)}, u32[]{:S(2)}) async-start(bf16[16,4,64,256]{3,2,1,0:T(8,128)(2,1)} %bitcast.44), calls=%async_computation.1 | async-start | bytes 4194304 | tf_op jit(solution)/shard_map/all_to_all | solution.py:119
  78.9 1.5 pad_maximum_fusion.3
  80.5 0.1 collective-permute-start.1
  80.6 0.2 copy-done.7
  80.8 0.2 pad_maximum_fusion.2
  81.0 0.3 collective-permute-start
  81.3 1.4 convolution_convert_fusion.4.q_ref
  82.7 1.6 multiply_convert_fusion
  84.3 0.4 collective-permute-done.1
  84.7 2.2 pad_maximum_fusion.1
  86.9 0.8 collective-permute-done
  87.7 2.3 pad_maximum_fusion
  90.0 31.5 %all-to-all-done.1 = bf16[16,4,64,256]{3,2,1,0:T(8,128)(2,1)} async-done(((bf16[16,4,64,256]{3,2,1,0:T(8,128)(2,1)}), bf16[16,4,64,256]{3,2,1,0:T(8,128)(2,1)}, u32[]{:S(2)}, u32[]{:S(2)}) %all-to-all-start.1) | async-done | bytes 2097184 | tf_op jit(solution)/shard_map/all_to_all | solution.py:119
  121.5 12.8 %attend.1 = (bf16[512,256]{1,0:T(8,128)(2,1)}, bf16[512,256]{1,0:T(8,128)(2,1)}, bf16[64,64,256]{2,1,0:T(8,128)(2,1)}, bf16[64,64,256]{2,1,0:T(8,128)(2,1)}) custom-call(s32[32]{0:T(128)} %copy-done.12, bf16[512,256]{1,0:T(8,128)(2,1)} %convolution_convert_fusion.4.q_ref, f32[512,256]{1,0:T(8,128)} %get-tuple-element.26.gate_ref, bf16[512,256]{1,0:T(8,128)(2,1)} %up_ref.1, ...), custom_call_target="tpu_custom_call" | custom-call | flops 2000000000 | bytes 8000000 | tf_op jit(solution)/shard_map/attend/pallas_call | solution.py:144
  134.3 58.1 %all_to_all.39 = bf16[16,4,64,256]{3,2,1,0:T(8,128)(2,1)} all-to-all(bf16[16,4,64,256]{3,2,1,0:T(8,128)(2,1)} %bitcast.49), channel_id=1, replica_groups=mesh['st'=16,'tp'=2] {'st'}, dimensions={0} | all-to-all | bytes 4194304 | tf_op jit(solution)/shard_map/all_to_all | solution.py:170
  192.5 4.4 %all-to-all-start.3 = ((bf16[16,4,64,256]{3,2,1,0:T(8,128)(2,1)}), bf16[16,4,64,256]{3,2,1,0:T(8,128)(2,1)}, u32[]{:S(2)}, u32[]{:S(2)}) async-start(bf16[16,4,64,256]{3,2,1,0:T(8,128)(2,1)} %bitcast.8), calls=%async_computation.3 | async-start | bytes 4194304 | tf_op jit(solution)/shard_map/all_to_all | solution.py:170
  196.9 0.6 select_n.57.passage_ref
  197.5 6.2 %totals.3 = bf16[32,64,256]{2,1,0:T(8,128)(2,1)} custom-call(s32[64]{0:T(128)} %select_n.57.passage_ref, bf16[64,64,256]{2,1,0:T(8,128)(2,1)} %bitcast.50), custom_call_target="tpu_custom_call" | custom-call | flops 1000000000 | bytes 4000000 | tf_op jit(solution)/shard_map/totals/pallas_call | solution.py:174
  203.7 6.1 %fusion.4 = bf16[32,16,8,128]{3,2,1,0:T(8,128)(2,1)S(1)} fusion(bf16[32,64,256]{2,1,0:T(8,128)(2,1)} %totals.3, bf16[32,64,2048]{2,1,0:T(8,128)(2,1)} %param.9), kind=kOutput, calls=%fused_computation.19 | convolution fusion | flops 2148007936 | bytes 10485760 | tf_op jit(solution)/shard_map/dot_general | solution.py:205
  209.8 1.2 copy.26
  211.0 28.0 %all-to-all-done.3 = bf16[16,4,64,256]{3,2,1,0:T(8,128)(2,1)} async-done(((bf16[16,4,64,256]{3,2,1,0:T(8,128)(2,1)}), bf16[16,4,64,256]{3,2,1,0:T(8,128)(2,1)}, u32[]{:S(2)}, u32[]{:S(2)}) %all-to-all-start.3) | async-done | bytes 2097184 | tf_op jit(solution)/shard_map/all_to_all | solution.py:170
  239.0 9.8 %all-to-all-start.5 = ((bf16[16,128,256]{1,2,0:T(8,128)(2,1)}), bf16[16,128,256]{1,2,0:T(8,128)(2,1)S(1)}, u32[]{:S(2)}, u32[]{:S(2)}) async-start(bf16[16,128,256]{1,2,0:T(8,128)(2,1)} %bitcast.41), calls=%async_computation.5 | async-start | bytes 2097152 | tf_op jit(solution)/shard_map/all_to_all | solution.py:206
  248.9 6.2 %totals.2 = bf16[32,64,256]{2,1,0:T(8,128)(2,1)} custom-call(s32[64]{0:T(128)} %select_n.57.passage_ref, bf16[64,64,256]{2,1,0:T(8,128)(2,1)} %bitcast.9.came_ref), custom_call_target="tpu_custom_call" | custom-call | flops 1000000000 | bytes 4000000 | tf_op jit(solution)/shard_map/totals/pallas_call | solution.py:174
  255.1 2.7 fusion.6
  257.8 14.7 %all-to-all-done.5 = bf16[16,128,256]{1,2,0:T(8,128)(2,1)S(1)} async-done(((bf16[16,128,256]{1,2,0:T(8,128)(2,1)}), bf16[16,128,256]{1,2,0:T(8,128)(2,1)S(1)}, u32[]{:S(2)}, u32[]{:S(2)}) %all-to-all-start.5) | async-done | bytes 1048608 | tf_op jit(solution)/shard_map/all_to_all | solution.py:206
  272.5 0.1 reduce_sum.32
  272.7 0.1 copy.22
  272.8 1.1 broadcast_in_dim.18
  273.9 5.9 %all-to-all-start.6 = ((bf16[16,128,256]{2,1,0:T(8,128)(2,1)}), bf16[16,128,256]{2,1,0:T(8,128)(2,1)S(1)}, u32[]{:S(2)}, u32[]{:S(2)}) async-start(bf16[16,128,256]{2,1,0:T(8,128)(2,1)} %broadcast_in_dim.18), calls=%async_computation.6 | async-start | bytes 2097152 | tf_op jit(solution)/shard_map/all_to_all | solution.py:213
  279.9 1.5 collective-permute-done.2
  281.5 4.6 %convolution_convert_fusion.1 = bf16[256,2048]{1,0:T(8,128)(2,1)} fusion(bf16[2048,1024]{1,0:T(8,128)(2,1)} %pad_maximum_fusion, bf16[256,512]{1,0:T(8,128)(2,1)S(1)} %collective-permute-done.2, bf16[256,512]{1,0:T(8,128)(2,1)S(1)} %get-tuple-element.21), kind=kOutput, calls=%fused_computation.6 | convolution fusion | flops 1075314688 | bytes 5767168 | tf_op jit(solution)/shard_map/dot_general | solution.py:200
  286.1 7.5 %convolution_convert_fusion = bf16[1024,2048]{1,0:T(8,128)(2,1)} fusion(bf16[2048,1024]{1,0:T(8,128)(2,1)S(1)} %copy-done.3, bf16[1024,512]{1,0:T(8,128)(2,1)} %collective-permute-done.3, bf16[1024,512]{1,0:T(8,128)(2,1)S(1)} %copy-done.8), kind=kOutput, calls=%fused_computation.4 | convolution fusion | flops 4301258752 | bytes 10485760 | tf_op jit(solution)/shard_map/dot_general | solution.py:200
  293.6 9.2 %all-to-all-done.6 = bf16[16,128,256]{2,1,0:T(8,128)(2,1)S(1)} async-done(((bf16[16,128,256]{2,1,0:T(8,128)(2,1)}), bf16[16,128,256]{2,1,0:T(8,128)(2,1)S(1)}, u32[]{:S(2)}, u32[]{:S(2)}) %all-to-all-start.6) | async-done | bytes 1048608 | tf_op jit(solution)/shard_map/all_to_all | solution.py:213
  302.7 1.5 bitcast_convert_fusion
  (35 shorter events, 0.3 us)
Async XLA Ops:
  0.6 80.7 %copy-start = (bf16[512,2048]{1,0:T(8,128)(2,1)S(1)}, bf16[512,2048]{1,0:T(8,128)(2,1)}, u32[]{:S(2)}) copy-start(bf16[512,2048]{1,0:T(8,128)(2,1)} %param.8) | copy-start | bytes 6291460
  1.8 15.1 %copy-start.12 = (s32[32]{0:T(128)}, s32[32]{0:T(128)S(1)}, u32[]{:S(2)}) copy-start(s32[32]{0:T(128)S(1)} %multiply_add_fusion.flat_ref) | copy-start | bytes 388
  2.6 15.6 %all-to-all-start = ((s32[16,1,4]{2,1,0:T(1,128)}), s32[16,1,4]{2,1,0:T(1,128)S(1)}, u32[]{:S(2)}, u32[]{:S(2)}) async-start(s32[16,1,4]{2,1,0:T(1,128)} %bitcast.2), calls=%async_computation | async-start | bytes 16384 | tf_op jit(solution)/shard_map/all_to_all | solution.py:105
  20.4 48.5 %all-to-all-start.2 = ((bf16[16,4,64,256]{3,2,1,0:T(8,128)(2,1)}), bf16[16,4,64,256]{3,2,1,0:T(8,128)(2,1)}, u32[]{:S(2)}, u32[]{:S(2)}) async-start(bf16[16,4,64,256]{3,2,1,0:T(8,128)(2,1)} %bitcast.45), calls=%async_computation.2 | async-start | bytes 4194304 | tf_op jit(solution)/shard_map/all_to_all | solution.py:123
  68.9 10.0 %copy-start.4 = (bf16[2048,256]{1,0:T(8,128)(2,1)S(1)}, bf16[2048,256]{1,0:T(8,128)(2,1)}, u32[]{:S(2)}) copy-start(bf16[2048,256]{1,0:T(8,128)(2,1)} %param.13) | copy-start | bytes 3145732
  68.9 52.6 %all-to-all-start.1 = ((bf16[16,4,64,256]{3,2,1,0:T(8,128)(2,1)}), bf16[16,4,64,256]{3,2,1,0:T(8,128)(2,1)}, u32[]{:S(2)}, u32[]{:S(2)}) async-start(bf16[16,4,64,256]{3,2,1,0:T(8,128)(2,1)} %bitcast.44), calls=%async_computation.1 | async-start | bytes 4194304 | tf_op jit(solution)/shard_map/all_to_all | solution.py:119
  78.9 1.6 copy-start.6
  78.9 1.8 copy-start.7
  80.5 4.2 %collective-permute-start.1 = (bf16[2048,512]{1,0:T(8,128)(2,1)S(1)}, bf16[2048,512]{1,0:T(8,128)(2,1)S(1)}, u32[]{:S(2)}, u32[]{:S(2)}) collective-permute-start(bf16[2048,512]{1,0:T(8,128)(2,1)S(1)} %pad_maximum_fusion.3), channel_id=1, source_target_pairs={{0,1},{1,0},{2,3},{3,2},{4,5},{5,4},{6,7},{7,6},{8,9},{9,8},{10,11... | collective-permute-start | bytes 6291464 | tf_op jit(solution)/shard_map/ppermute | solution.py:136
  80.9 1.8 copy-start.11
  81.0 6.7 %collective-permute-start = (bf16[2048,512]{1,0:T(8,128)(2,1)S(1)}, bf16[2048,512]{1,0:T(8,128)(2,1)S(1)}, u32[]{:S(2)}, u32[]{:S(2)}) collective-permute-start(bf16[2048,512]{1,0:T(8,128)(2,1)S(1)} %pad_maximum_fusion.2), channel_id=1, source_target_pairs={{0,1},{1,0},{2,3},{3,2},{4,5},{5,4},{6,7},{7,6},{8,9},{9,8},{10,11... | collective-permute-start | bytes 6291464 | tf_op jit(solution)/shard_map/ppermute | solution.py:133
  82.7 2.0 copy-start.5
  192.5 46.5 %all-to-all-start.3 = ((bf16[16,4,64,256]{3,2,1,0:T(8,128)(2,1)}), bf16[16,4,64,256]{3,2,1,0:T(8,128)(2,1)}, u32[]{:S(2)}, u32[]{:S(2)}) async-start(bf16[16,4,64,256]{3,2,1,0:T(8,128)(2,1)} %bitcast.8), calls=%async_computation.3 | async-start | bytes 4194304 | tf_op jit(solution)/shard_map/all_to_all | solution.py:170
  239.0 33.5 %all-to-all-start.5 = ((bf16[16,128,256]{1,2,0:T(8,128)(2,1)}), bf16[16,128,256]{1,2,0:T(8,128)(2,1)S(1)}, u32[]{:S(2)}, u32[]{:S(2)}) async-start(bf16[16,128,256]{1,2,0:T(8,128)(2,1)} %bitcast.41), calls=%async_computation.5 | async-start | bytes 2097152 | tf_op jit(solution)/shard_map/all_to_all | solution.py:206
  248.8 6.2 %copy-start.2 = (bf16[32,64,256]{2,1,0:T(8,128)(2,1)S(1)}, bf16[32,64,256]{2,1,0:T(8,128)(2,1)}, u32[]{:S(2)}) copy-start(bf16[32,64,256]{2,1,0:T(8,128)(2,1)} %totals.3) | copy-start | bytes 3145732
  257.8 22.0 %copy-start.10 = (bf16[512,256]{1,0:T(8,128)(2,1)S(1)}, bf16[512,256]{1,0:T(8,128)(2,1)}, u32[]{:S(2)}) copy-start(bf16[512,256]{1,0:T(8,128)(2,1)} %get-tuple-element.11) | copy-start | bytes 786436
  257.8 28.3 %collective-permute-start.3 = (bf16[1024,512]{1,0:T(8,128)(2,1)}, bf16[1024,512]{1,0:T(8,128)(2,1)}, u32[]{:S(2)}, u32[]{:S(2)}) collective-permute-start(bf16[1024,512]{1,0:T(8,128)(2,1)} %get-tuple-element.20), channel_id=1, source_target_pairs={{0,1},{1,0},{2,3},{3,2},{4,5},{5,4},{6,7},{7,6},{8,9},{9,8},{10,11... | collective-permute-start | bytes 3145736 | tf_op jit(solution)/shard_map/ppermute | solution.py:198
  272.7 7.1 %copy-start.9 = (bf16[512,256]{1,0:T(8,128)(2,1)S(1)}, bf16[512,256]{1,0:T(8,128)(2,1)}, u32[]{:S(2)}) copy-start(bf16[512,256]{1,0:T(8,128)(2,1)} %get-tuple-element.12) | copy-start | bytes 786436
  273.9 28.8 %all-to-all-start.6 = ((bf16[16,128,256]{2,1,0:T(8,128)(2,1)}), bf16[16,128,256]{2,1,0:T(8,128)(2,1)S(1)}, u32[]{:S(2)}, u32[]{:S(2)}) async-start(bf16[16,128,256]{2,1,0:T(8,128)(2,1)} %broadcast_in_dim.18), calls=%async_computation.6 | async-start | bytes 2097152 | tf_op jit(solution)/shard_map/all_to_all | solution.py:213
  279.9 1.6 collective-permute-start.2
  281.5 4.6 %copy-start.3 = (bf16[2048,1024]{1,0:T(8,128)(2,1)S(1)}, bf16[2048,1024]{1,0:T(8,128)(2,1)}, u32[]{:S(2)}) copy-start(bf16[2048,1024]{1,0:T(8,128)(2,1)} %pad_maximum_fusion.1) | copy-start | bytes 12582916
  281.5 4.6 %copy-start.8 = (bf16[1024,512]{1,0:T(8,128)(2,1)S(1)}, bf16[1024,512]{1,0:T(8,128)(2,1)}, u32[]{:S(2)}) copy-start(bf16[1024,512]{1,0:T(8,128)(2,1)} %get-tuple-element.19) | copy-start | bytes 3145732
  286.1 18.2 %copy-start.1 = (bf16[512,2048]{1,0:T(8,128)(2,1)S(1)}, bf16[512,2048]{1,0:T(8,128)(2,1)}, u32[]{:S(2)}) copy-start(bf16[512,2048]{1,0:T(8,128)(2,1)} %param.8) | copy-start | bytes 6291460
